TPU v7x, 32 devices: a whole 2x2x4 slice. The times are simulated.
32 devices in a mesh: sp: 8 (over z, core), tp: 4 (over y, x).
Axes of the slice: x: 2, y: 2, z: 4, core: 2. Of those that a mesh axis runs over, the one named last changes fastest.
Arguments:
- residual_input: bfloat16 [1024, 2048], P(('sp', 'tp')), may hold values from -6 to 6
- mixer_value_input: bfloat16 [1024, 2048], P('sp', 'tp'), may hold values from -6 to 6
- gate_preactivation: bfloat16 [1024, 2048], P('sp', 'tp'), may hold values from -6 to 6
- state_projection_input: bfloat16 [1024, 2, 4, 128], P('sp'), may hold values from -6 to 6
- step_preactivation: bfloat16 [1024, 2, 32], P('sp', None, 'tp'), may hold values from -6 to 6
- spike_log_decay: float32 [1024, 2, 32], P('sp', None, 'tp'), may hold values from -1 to 0
- value_filter_taps: float32 [5, 2048], P(None, 'tp'), may hold values from -2.5 to 2.5
- state_projection_taps: float32 [5, 2, 4, 128], replicated, may hold values from -2.5 to 2.5
- step_size_bias: float32 [2, 32], P(None, 'tp'), may hold values from -0.5 to 0.5
- head_log_decay: float32 [2, 32], P(None, 'tp'), may hold values from -12 to -3
- gated_norm_gain: float32 [2048], P('tp'), may hold values from 0.1 to 1.9
- mixer_output_weight: bfloat16 [2048, 2048], P('tp'), may hold values from -0.125 to 0.125
- feedforward_norm_gain: float32 [2048], replicated, may hold values from 0.1 to 1.9
- routed_expert_index: int32 [1024, 4], P('sp'), may hold values from 0 to 7, all different within a row; in each aligned block of 128 rows (0 to 127, 128 to 255, ...) at most 96 rows name the same one
- routed_expert_weight: float32 [1024, 4], P('sp'), may hold values from 0.2 to 1.2
- routed_gate_weight: bfloat16 [8, 2048, 2048], P('sp', None, 'tp'), may hold values from -0.125 to 0.125
- routed_up_weight: bfloat16 [8, 2048, 2048], P('sp', None, 'tp'), may hold values from -0.125 to 0.125
- routed_down_weight: bfloat16 [8, 2048, 2048], P('sp', 'tp'), may hold values from -0.1875 to 0.1875
- common_gate_weight: bfloat16 [2048, 2048], P(None, 'tp'), may hold values from -0.125 to 0.125
- common_up_weight: bfloat16 [2048, 2048], P(None, 'tp'), may hold values from -0.125 to 0.125
- common_down_weight: bfloat16 [2048, 2048], P('tp'), may hold values from -0.125 to 0.125
Outputs:
- layer_out: bfloat16 [1024, 2048], P(('sp', 'tp'))
Inputs may be any that keep to these rules, and one draw needn't show every extreme that they name: `routed_expert_index`: each row names 4 different experts. In the aligned blocks of 128 rows no expert is named by more than 96 rows, and in some block one expert is named by exactly 96.
All inputs are finite; a program needn't handle non-finite values.
Results may differ from a plain program's by a relative error of at most 0.02.
Values may be sent and summed in bfloat16 or wider, within the bound.
A program may use at most 64 MiB of HBM per device.

v0:
```python
import jax
import jax.numpy as jnp
from jax import lax
from jax.sharding import PartitionSpec as P

HD = 64
BLK = 128


EPSILON = 1e-06
HIGHEST = lax.Precision.HIGHEST


def padded_2(cells, sides, width):
    for axis, dim in sides:
        count = lax.axis_size(axis)
        ends = count - 1
        head = lax.slice_in_dim(cells, 0, width, axis=dim)
        tail = lax.slice_in_dim(cells, cells.shape[dim] - width, cells.shape[dim], axis=dim)
        cells = jnp.concatenate(
            [
                lax.ppermute(tail, axis, [(i, (i + 1) % count) for i in range(ends)]),
                cells,
                lax.ppermute(head, axis, [((i + 1) % count, i) for i in range(ends)]),
            ],
            axis=dim,
        )
    return cells


def rounded(values):
    return lax.optimization_barrier(values.astype(jnp.bfloat16)).astype(jnp.float32)


def block_pass(inputs, decay_logarithm, b_state, c_state, block_len):
    length, groups, per_group, head_dim = inputs.shape
    states = b_state.shape[-1]
    blocks = length // block_len
    inputs = inputs.reshape(blocks, block_len, groups, per_group, head_dim)
    decay_logarithm = decay_logarithm.reshape(blocks, block_len, groups, per_group)
    b_blocks = b_state.reshape(blocks, block_len, groups, states)
    c_blocks = c_state.reshape(blocks, block_len, groups, states)
    within = jnp.cumsum(decay_logarithm, axis=1)
    row_index = lax.broadcasted_iota(jnp.int32, (block_len, block_len), 0)
    col_index = lax.broadcasted_iota(jnp.int32, (block_len, block_len), 1)
    below_mask = (row_index >= col_index)[None, :, :, None, None]
    spread = within[:, :, None] - within[:, None, :]
    weights = jnp.where(below_mask, jnp.exp(jnp.where(below_mask, spread, 0.0)), 0.0)
    scores = jnp.einsum("cign,cjgn->cijg", c_blocks, b_blocks, precision=HIGHEST)
    output = jnp.einsum(
        "cijgr,cjgrp->cigrp", scores[..., None] * weights, inputs, precision=HIGHEST
    )
    tail_decay = jnp.exp(within[:, -1:] - within)
    block_ends = jnp.einsum(
        "cjgn,cjgrp->cgrpn", b_blocks, inputs * tail_decay[..., None], precision=HIGHEST
    )
    totals = within[:, -1]

    def carry_step(carried, pair_item):
        block_total, block_end = pair_item
        return (jnp.exp(block_total)[..., None, None] * carried + block_end, carried)

    zero_state = jnp.zeros((groups, per_group, head_dim, states), jnp.float32)
    last_state, starts = lax.scan(carry_step, zero_state, (totals, block_ends))
    output = (
        output
        + jnp.einsum("cign,cgrpn->cigrp", c_blocks, starts, precision=HIGHEST)
        * jnp.exp(within)[..., None]
    )
    offsets = jnp.cumsum(totals, axis=0) - totals
    through = (within + offsets[:, None]).reshape(length, groups, per_group)
    return (
        output.reshape(length, groups, per_group, head_dim),
        jnp.sum(totals, axis=0),
        last_state,
        through,
    )


def slot_table(expert_ids, experts, capacity):
    row_count, top_count = expert_ids.shape
    flat_ids = expert_ids.reshape(-1)
    one_hot = (flat_ids[:, None] == jnp.arange(experts, dtype=jnp.int32)[None, :]).astype(jnp.int32)
    earlier = jnp.cumsum(one_hot, axis=0) - one_hot
    position = jnp.sum(earlier * one_hot, axis=1)
    owners = jnp.arange(row_count * top_count, dtype=jnp.int32) // top_count
    table = (
        jnp.full((experts * capacity,), row_count, jnp.int32)
        .at[flat_ids * capacity + position]
        .set(owners)
    )
    return (position.reshape(row_count, top_count), table)


def on_device(
    residual_input,
    mixer_value_input,
    gate_preactivation,
    state_projection_input,
    step_preactivation,
    spike_log_decay,
    value_filter_taps,
    state_projection_taps,
    step_size_bias,
    head_log_decay,
    gated_norm_gain,
    mixer_output_weight,
    feedforward_norm_gain,
    routed_expert_index,
    routed_expert_weight,
    routed_gate_weight,
    routed_up_weight,
    routed_down_weight,
    common_gate_weight,
    common_up_weight,
    common_down_weight,
):
    seq_rows, mixer_cols = mixer_value_input.shape
    heads_dev = mixer_cols // HD
    groups, states = (state_projection_input.shape[2], state_projection_input.shape[3])
    per_group = heads_dev * lax.axis_size("tp") // groups
    group_count = max(1, heads_dev // per_group)
    heads_local = heads_dev // group_count
    first_group = lax.axis_index("tp") * heads_dev // per_group
    taps = value_filter_taps.shape[0]
    margin = taps // 2
    local_bc = lax.dynamic_slice_in_dim(state_projection_input, first_group, group_count, 2)
    local_taps = lax.dynamic_slice_in_dim(state_projection_taps, first_group, group_count, 2)
    joined = jnp.concatenate(
        [mixer_value_input, local_bc.reshape(seq_rows, 2 * group_count * states)], axis=1
    )
    kernel = jnp.concatenate(
        [value_filter_taps, local_taps.reshape(taps, 2 * group_count * states)], axis=1
    )
    padded = padded_2(joined, (("sp", 0),), margin)
    conv_out = jnp.zeros(joined.shape, jnp.float32)
    for offset in range(taps):
        conv_out = conv_out + kernel[offset] * padded[offset : offset + seq_rows].astype(
            jnp.float32
        )
    active = jax.nn.silu(conv_out)
    mixer_values = active[:, :mixer_cols].reshape(seq_rows, group_count, heads_local, HD)
    state_parts = active[:, mixer_cols:].reshape(seq_rows, 2, group_count, states)
    b_state, c_state = (state_parts[:, 0], state_parts[:, 1])
    discrete_step_size = jax.nn.softplus(step_preactivation.astype(jnp.float32) + step_size_bias)
    decay_logarithm = spike_log_decay - discrete_step_size * jnp.exp(head_log_decay)
    forward_in = (
        mixer_values
        * discrete_step_size[:, 0].reshape(seq_rows, group_count, heads_local)[..., None]
    )
    backward_in = (
        mixer_values
        * discrete_step_size[:, 1].reshape(seq_rows, group_count, heads_local)[..., None]
    )
    forward_out, forward_total, forward_end, forward_through = block_pass(
        forward_in,
        decay_logarithm[:, 0].reshape(seq_rows, group_count, heads_local),
        b_state,
        c_state,
        BLK,
    )
    backward_out, backward_total, backward_end, backward_through = block_pass(
        jnp.flip(backward_in, 0),
        jnp.flip(decay_logarithm[:, 1].reshape(seq_rows, group_count, heads_local), 0),
        jnp.flip(b_state, 0),
        jnp.flip(c_state, 0),
        BLK,
    )
    totals_fwd, ends_fwd, totals_bwd, ends_bwd = (
        lax.all_gather(forward_total[None].astype(jnp.bfloat16), "sp", axis=0, tiled=True).astype(
            jnp.float32
        ),
        lax.all_gather(forward_end[None].astype(jnp.bfloat16), "sp", axis=0, tiled=True).astype(
            jnp.float32
        ),
        lax.all_gather(backward_total[None].astype(jnp.bfloat16), "sp", axis=0, tiled=True).astype(
            jnp.float32
        ),
        lax.all_gather(backward_end[None].astype(jnp.bfloat16), "sp", axis=0, tiled=True).astype(
            jnp.float32
        ),
    )
    device = lax.axis_index("sp")
    order = jnp.arange(totals_fwd.shape[0], dtype=jnp.int32)[:, None, None]
    before_fwd = jnp.cumsum(totals_fwd, axis=0) - totals_fwd
    own_fwd = lax.dynamic_index_in_dim(before_fwd, device, 0, keepdims=True)
    lower_mask = order < device
    exponent_fwd = jnp.where(lower_mask, own_fwd - before_fwd - totals_fwd, 0.0)
    weight_fwd = jnp.where(lower_mask, jnp.exp(exponent_fwd), 0.0)
    forward_start = jnp.einsum("sgr,sgrpn->grpn", weight_fwd, ends_fwd, precision=HIGHEST)
    before_bwd = jnp.cumsum(totals_bwd, axis=0) - totals_bwd
    own_bwd = lax.dynamic_index_in_dim(before_bwd, device, 0, keepdims=True)
    own_total = lax.dynamic_index_in_dim(totals_bwd, device, 0, keepdims=True)
    upper_mask = order > device
    exponent_bwd = jnp.where(upper_mask, before_bwd - own_bwd - own_total, 0.0)
    weight_bwd = jnp.where(upper_mask, jnp.exp(exponent_bwd), 0.0)
    backward_start = jnp.einsum("sgr,sgrpn->grpn", weight_bwd, ends_bwd, precision=HIGHEST)
    forward_out = forward_out + jnp.exp(forward_through)[..., None] * jnp.einsum(
        "lgn,grpn->lgrp", c_state, forward_start, precision=HIGHEST
    )
    backward_out = backward_out + jnp.exp(backward_through)[..., None] * jnp.einsum(
        "lgn,grpn->lgrp", jnp.flip(c_state, 0), backward_start, precision=HIGHEST
    )
    scanned = (forward_out + jnp.flip(backward_out, 0)).reshape(seq_rows, mixer_cols)
    gated = (scanned * jax.nn.silu(gate_preactivation.astype(jnp.float32))).reshape(
        seq_rows, heads_dev, HD
    )
    gated = gated * lax.rsqrt(jnp.mean(gated * gated, axis=-1, keepdims=True) + EPSILON)
    mixed = (gated.reshape(seq_rows, mixer_cols) * gated_norm_gain).astype(jnp.bfloat16)
    picked_rows = mixed
    projected = lax.psum_scatter(
        rounded(
            jnp.dot(picked_rows, mixer_output_weight, preferred_element_type=jnp.float32)
        ).astype(jnp.bfloat16),
        "tp",
        scatter_dimension=0,
        tiled=True,
    ).astype(jnp.float32)
    residual = (residual_input.astype(jnp.float32) + projected).astype(jnp.bfloat16)
    widened = residual.astype(jnp.float32)
    normed = (
        widened
        * lax.rsqrt(jnp.mean(widened * widened, axis=-1, keepdims=True) + EPSILON)
        * feedforward_norm_gain
    ).astype(jnp.bfloat16)
    all_rows = lax.all_gather(normed, "tp", axis=0, tiled=True)
    sp_count = lax.axis_size("sp")
    local_experts = routed_gate_weight.shape[0]
    experts = local_experts * sp_count
    top_count = routed_expert_index.shape[1]
    capacity = 3 * seq_rows * top_count // (2 * experts)
    model_width = all_rows.shape[1]
    position, table = slot_table(routed_expert_index, experts, capacity)
    padded_rows = jnp.concatenate([all_rows, jnp.zeros((1, model_width), jnp.bfloat16)], axis=0)
    outgoing = padded_rows[table].reshape(sp_count, local_experts, capacity, model_width)
    arrived = lax.all_to_all(outgoing, "sp", split_axis=0, concat_axis=0, tiled=True)
    gate_part = jnp.einsum(
        "secd,edf->secf", arrived, routed_gate_weight, preferred_element_type=jnp.float32
    )
    up_part = jnp.einsum(
        "secd,edf->secf", arrived, routed_up_weight, preferred_element_type=jnp.float32
    )
    hidden = (jax.nn.silu(gate_part) * up_part).astype(jnp.bfloat16)
    partial_value = lax.optimization_barrier(
        jnp.einsum(
            "secf,efd->secd", hidden, routed_down_weight, preferred_element_type=jnp.float32
        ).astype(jnp.bfloat16)
    ).astype(jnp.float32)
    summed = lax.psum_scatter(
        partial_value.astype(jnp.bfloat16), "tp", scatter_dimension=3, tiled=True
    ).astype(jnp.float32)
    returned = lax.all_to_all(
        summed.astype(jnp.bfloat16), "sp", split_axis=0, concat_axis=0, tiled=True
    ).astype(summed.dtype)
    slot_index = routed_expert_index * capacity + position
    flat_back = returned.reshape(experts * capacity, returned.shape[3])
    chosen = flat_back[slot_index]
    routed = jnp.sum(routed_expert_weight[..., None] * chosen, axis=1)
    routed_part = lax.all_to_all(
        routed.astype(jnp.bfloat16), "tp", split_axis=0, concat_axis=1, tiled=True
    ).astype(routed.dtype)
    picked_rows = all_rows
    gate_part = jnp.dot(picked_rows, common_gate_weight, preferred_element_type=jnp.float32)
    up_part = jnp.dot(picked_rows, common_up_weight, preferred_element_type=jnp.float32)
    hidden = (jax.nn.silu(gate_part) * up_part).astype(jnp.bfloat16)
    shared_part = lax.psum_scatter(
        rounded(jnp.dot(hidden, common_down_weight, preferred_element_type=jnp.float32)).astype(
            jnp.bfloat16
        ),
        "tp",
        scatter_dimension=0,
        tiled=True,
    ).astype(jnp.float32)
    feed = shared_part + routed_part
    return (widened + feed).astype(jnp.bfloat16)


def solution(mesh):
    return jax.shard_map(
        on_device,
        mesh=mesh,
        in_specs=(
            P(("sp", "tp"), None),
            P("sp", "tp"),
            P("sp", "tp"),
            P("sp", None, None, None),
            P("sp", None, "tp"),
            P("sp", None, "tp"),
            P(None, "tp"),
            P(),
            P(None, "tp"),
            P(None, "tp"),
            P("tp"),
            P("tp", None),
            P(),
            P("sp", None),
            P("sp", None),
            P("sp", None, "tp"),
            P("sp", None, "tp"),
            P("sp", "tp", None),
            P(None, "tp"),
            P(None, "tp"),
            P("tp", None),
        ),
        out_specs=P(("sp", "tp"), None),
        check_vma=False,
    )
```

profile of v0, /device:TPU:0, one launch (start us, length us, event | category | flops | bytes accessed | tf_op | source)
XLA Modules:
  0.0 322.3 jit_solution(15125792597423114408)
XLA Ops:
  6.5 1.2 constant_dynamic-slice_fusion.3
  7.9 1.0 copy.98
  9.1 2.4 collective-permute-start
  11.5 1.3 collective-permute-start.1
  12.8 0.7 exp.116
  13.5 0.8 compare_select_fusion.1
  15.6 0.8 dynamic-slice_reduce_fusion
  17.0 0.7 constant_dynamic-update-slice_fusion
  17.7 15.3 %all-gather.2 = bf16[8,1,1,8]{3,2,1,0:T(2,128)(2,1)S(1)} all-gather(bf16[1,1,1,8]{3,2,1,0:T(2,128)(2,1)S(1)} %slice.182), channel_id=4, replica_groups=mesh['sp'=8,'tp'=4] {'sp'}, dimensions={0}, use_global_device_ids=true | all-gather | bytes 144 | tf_op jit(solution)/shard_map/all_gather | solution.py:176
  35.0 8.7 %all-gather = bf16[8,1,1,8]{3,2,1,0:T(2,128)(2,1)S(1)} all-gather(bf16[1,1,1,8]{3,2,1,0:T(2,128)(2,1)S(1)} %slice.183), channel_id=2, replica_groups=mesh['sp'=8,'tp'=4] {'sp'}, dimensions={0}, use_global_device_ids=true | all-gather | bytes 144 | tf_op jit(solution)/shard_map/all_gather | solution.py:170
  43.9 1.2 divide_multiply_fusion
  46.0 0.7 broadcast_multiply_fusion
  46.9 1.7 fusion.33
  48.9 0.7 fusion.109
  49.7 0.8 copy.113
  50.6 2.1 reduce-window.6
  52.7 1.0 fusion.32
  54.7 1.1 fusion.29
  55.8 2.7 fusion.22
  58.8 1.9 fusion.24
  60.7 9.5 %all-gather.9.cloned.1.call-done = bf16[64,64,128]{2,1,0:T(8,128)(2,1)} async-done(((bf16[8,64,128]{2,1,0:T(8,128)(2,1)}), bf16[64,64,128]{2,1,0:T(8,128)(2,1)}) %all-gather.9.cloned.1.call-update) | async-done | bytes 1048592 | tf_op jit(solution)/shard_map/all_gather | solution.py:179
  70.3 2.5 fusion.35
  73.3 20.5 %all-gather.7.cloned.1.call-done = bf16[64,64,128]{2,1,0:T(8,128)(2,1)} async-done(((bf16[8,64,128]{2,1,0:T(8,128)(2,1)}), bf16[64,64,128]{2,1,0:T(8,128)(2,1)}) %all-gather.7.cloned.1.call-update) | async-done | bytes 1048592 | tf_op jit(solution)/shard_map/all_gather | solution.py:173
  93.8 2.5 fusion.37
  97.3 2.9 convolution_convert_fusion.2
  101.8 2.4 scatter_custom_fusion
  104.3 20.8 %reduce-scatter.4.cloned.1.call-done = bf16[32,2048]{1,0:T(8,128)(2,1)} async-done(((bf16[128,2048]{1,0:T(8,128)(2,1)}), bf16[32,2048]{1,0:T(8,128)(2,1)}) %reduce-scatter.4.cloned.1.call-update) | async-done | bytes 131088 | tf_op jit(solution)/shard_map/reduce_scatter | solution.py:211
  125.1 1.1 fusion.58
  126.2 1.0 fusion.60
  127.2 10.3 %all_gather.19 = bf16[128,2048]{1,0:T(8,128)(2,1)S(1)} all-gather(bf16[32,2048]{1,0:T(8,128)(2,1)S(1)} %fusion.60), channel_id=1, replica_groups=mesh['sp'=8,'tp'=4] {'tp'}, dimensions={0}, use_global_device_ids=true | all-gather | bytes 655360 | tf_op jit(solution)/shard_map/all_gather | solution.py:226
  137.5 4.3 %gather_fusion = bf16[768,2048]{1,0:T(8,128)(2,1)} fusion(bf16[129,2048]{1,0:T(8,128)(2,1)S(1)} %concatenate.22, s32[1024]{0:T(1024)S(1)} %pad_clamp_fusion.1), kind=kCustom, calls=%fused_computation | custom fusion | bytes 6294528 | tf_op jit(solution)/shard_map/gather | solution.py:235
  141.8 76.2 %all_to_all.20 = bf16[8,1,96,2048]{3,2,1,0:T(8,128)(2,1)S(1)} all-to-all(bf16[8,1,96,2048]{3,2,1,0:T(8,128)(2,1)} %bitcast.288), channel_id=1, replica_groups=mesh['sp'=8,'tp'=4] {'sp'}, dimensions={0} | all-to-all | bytes 6291456 | tf_op jit(solution)/shard_map/all_to_all | solution.py:236
  218.0 1.7 copy-done.1
  219.7 2.9 fusion.2
  222.6 8.1 %fusion.4 = bf16[8,1,96,2048]{3,2,0,1:T(8,128)(2,1)} fusion(bf16[1,512,2048]{2,1,0:T(8,128)(2,1)S(1)} %copy-done, bf16[1,2048,512]{2,1,0:T(8,128)(2,1)} %param.37, bf16[8,1,96,2048]{3,2,1,0:T(8,128)(2,1)} %copy-done.1, f32[8,96,512]{2,1,0:T(8,128)} %fusion.2), kind=kOutput, calls=%fused_computation.8 | convolution fusion | flops 3225157632 | bytes 12058624 | tf_op jit(solution)/shard_map/secf,efd->secd/dot_general | solution.py:245
  230.8 42.0 %reduce-scatter.8.cloned.1.call-done = bf16[8,1,96,512]{3,2,0,1:T(8,128)(2,1)} async-done(((bf16[8,1,96,2048]{3,2,0,1:T(8,128)(2,1)}), bf16[8,1,96,512]{3,2,0,1:T(8,128)(2,1)}) %reduce-scatter.8.cloned.1.call-update) | async-done | bytes 786448 | tf_op jit(solution)/shard_map/reduce_scatter | solution.py:249
  272.8 4.6 %all-to-all-start.1 = ((bf16[8,1,96,512]{3,2,1,0:T(8,128)(2,1)}), bf16[8,1,96,512]{3,2,1,0:T(8,128)(2,1)S(1)}, u32[]{:S(2)}, u32[]{:S(2)}) async-start(bf16[8,1,96,512]{3,2,1,0:T(8,128)(2,1)} %bitcast.307), calls=%async_computation.4 | async-start | bytes 1572864 | tf_op jit(solution)/shard_map/all_to_all | solution.py:252
  277.5 2.8 fusion.127
  280.3 4.0 %convolution_convert_fusion.1 = bf16[128,2048]{1,0:T(8,128)(2,1)} fusion(bf16[512,2048]{1,0:T(8,128)(2,1)} %param.41, bf16[128,2048]{1,0:T(8,128)(2,1)S(1)} %all_gather.19, bf16[2048,512]{1,0:T(8,128)(2,1)} %param.40, f32[128,512]{1,0:T(8,128)} %fusion.127), kind=kOutput, calls=%fused_computation.9 | convolution fusion | flops 537526272 | bytes 5505024 | tf_op jit(solution)/shard_map/dot_general | solution.py:267
  284.3 0.9 reshape.562
  285.2 0.7 copy.112
  286.0 12.4 %all-to-all-done.1 = bf16[8,1,96,512]{3,2,1,0:T(8,128)(2,1)S(1)} async-done(((bf16[8,1,96,512]{3,2,1,0:T(8,128)(2,1)}), bf16[8,1,96,512]{3,2,1,0:T(8,128)(2,1)S(1)}, u32[]{:S(2)}, u32[]{:S(2)}) %all-to-all-start.1) | async-done | bytes 786464 | tf_op jit(solution)/shard_map/all_to_all | solution.py:252
  298.4 1.4 bitcast_convert_fusion
  299.8 3.4 %gather_fusion.1 = f32[512,512]{1,0:T(8,128)S(1)} fusion(f32[768,512]{1,0:T(8,128)} %bitcast_convert_fusion, s32[1024]{0:T(1024)S(1)} %pad_clamp_fusion), kind=kCustom, calls=%fused_computation.1 | custom fusion | bytes 2099200 | tf_op jit(solution)/shard_map/gather | solution.py:257
  303.3 1.3 reshape.561
  304.6 2.0 multiply_reduce_fusion
  306.6 7.5 %all_to_all.21 = bf16[4,32,512]{2,1,0:T(8,128)(2,1)S(1)} all-to-all(bf16[4,32,512]{2,1,0:T(8,128)(2,1)S(1)} %bitcast.308), channel_id=1, replica_groups=mesh['sp'=8,'tp'=4] {'tp'}, dimensions={0} | all-to-all | bytes 262144 | tf_op jit(solution)/shard_map/all_to_all | solution.py:259
  314.2 1.6 fusion.61
  (122 shorter events, 10.2 us)
Async XLA Ops:
  6.5 216.1 %copy-start = (bf16[1,512,2048]{2,1,0:T(8,128)(2,1)S(1)}, bf16[1,512,2048]{2,1,0:T(8,128)(2,1)}, u32[]{:S(2)}) copy-start(bf16[1,512,2048]{2,1,0:T(8,128)(2,1)} %param.38) | copy-start | bytes 6291460
  6.5 63.7 %all-gather.9.cloned.1.call-start = ((), (), s32[]{:S(2)}) async-start(), calls=%async_computation.10 | async-start | bytes 1179648 | tf_op jit(solution)/shard_map/all_gather | solution.py:179
  9.1 34.6 %collective-permute-start = (bf16[2,768]{0,1:T(8,128)(2,1)S(1)}, bf16[2,768]{0,1:T(8,128)(2,1)S(1)}, u32[]{:S(2)}, u32[]{:S(2)}) collective-permute-start(bf16[2,768]{0,1:T(8,128)(2,1)S(1)} %get-tuple-element.44), channel_id=1, source_target_pairs={{0,4},{4,8},{8,12},{12,16},{16,20},{20,24},{24,28},{1,5},{5,9},{9,... | collective-permute-start | bytes 9224 | tf_op jit(solution)/shard_map/ppermute | solution.py:22
  11.5 32.2 %collective-permute-start.1 = (bf16[2,768]{0,1:T(8,128)(2,1)S(1)}, bf16[2,768]{0,1:T(8,128)(2,1)S(1)}, u32[]{:S(2)}, u32[]{:S(2)}) collective-permute-start(bf16[2,768]{0,1:T(8,128)(2,1)S(1)} %get-tuple-element.45), channel_id=1, source_target_pairs={{4,0},{8,4},{12,8},{16,12},{20,16},{24,20},{28,24},{5,1},{9,5},{13... | collective-permute-start | bytes 9224 | tf_op jit(solution)/shard_map/ppermute | solution.py:24
  15.3 19.7 %copy-start.9 = (f32[1,128,1,8]{1,3,2,0:T(8,128)}, f32[1,128,1,8]{1,3,2,0:T(8,128)S(1)}, u32[]{:S(2)}) copy-start(f32[1,128,1,8]{1,3,2,0:T(8,128)S(1)} %copy.107) | copy-start | bytes 12292
  15.6 18.7 %copy-start.10 = (f32[1,128,1,8]{1,3,2,0:T(8,128)}, f32[1,128,1,8]{1,3,2,0:T(8,128)S(1)}, u32[]{:S(2)}) copy-start(f32[1,128,1,8]{1,3,2,0:T(8,128)S(1)} %copy.103) | copy-start | bytes 12292
  17.0 29.0 %copy-start.8 = (f32[128,8]{0,1:T(8,128)}, f32[128,8]{0,1:T(8,128)S(1)}, u32[]{:S(2)}) copy-start(f32[128,8]{0,1:T(8,128)S(1)} %get-tuple-element.54) | copy-start | bytes 12292
  46.0 8.2 %copy-start.6 = (f32[128,1,1,128]{0,3,1,2:T(8,128)S(1)}, f32[128,1,1,128]{0,3,1,2:T(8,128)}, u32[]{:S(2)}) copy-start(f32[128,1,1,128]{0,3,1,2:T(8,128)} %get-tuple-element.47) | copy-start | bytes 196612
  46.9 11.6 %copy-start.11 = (f32[128,8]{0,1:T(8,128)S(1)}, f32[128,8]{0,1:T(8,128)}, u32[]{:S(2)}) copy-start(f32[128,8]{0,1:T(8,128)} %get-tuple-element.62) | copy-start | bytes 12292
  48.6 45.2 %all-gather.7.cloned.1.call-start = ((), (), s32[]{:S(2)}) async-start(), calls=%async_computation.9 | async-start | bytes 1179648 | tf_op jit(solution)/shard_map/all_gather | solution.py:173
  53.7 71.3 %reduce-scatter.4.cloned.1.call-start = ((), (), s32[]{:S(2)}) async-start(), calls=%async_computation.6 | async-start | bytes 655360 | tf_op jit(solution)/shard_map/reduce_scatter | solution.py:211
  58.4 14.3 %copy-start.5 = (f32[128,1,8,64]{0,3,2,1:T(8,128)S(1)}, f32[128,1,8,64]{0,3,2,1:T(8,128)}, u32[]{:S(2)}) copy-start(f32[128,1,8,64]{0,3,2,1:T(8,128)} %fusion.22) | copy-start | bytes 786436
  72.8 24.0 %copy-start.4 = (bf16[128,512]{1,0:T(8,128)(2,1)S(1)}, bf16[128,512]{1,0:T(8,128)(2,1)}, u32[]{:S(2)}) copy-start(bf16[128,512]{1,0:T(8,128)(2,1)} %param.23) | copy-start | bytes 393220
  96.3 1.0 copy-start.14
  97.1 3.3 %copy-start.7 = (s32[8,4,128]{2,0,1:T(8,128)S(1)}, s32[8,4,128]{2,0,1:T(8,128)}, u32[]{:S(2)}) copy-start(s32[8,4,128]{2,0,1:T(8,128)} %reduce-window.6) | copy-start | bytes 49156
  97.3 27.8 %copy-start.2 = (bf16[32,2048]{1,0:T(8,128)(2,1)S(1)}, bf16[32,2048]{1,0:T(8,128)(2,1)}, u32[]{:S(2)}) copy-start(bf16[32,2048]{1,0:T(8,128)(2,1)} %param.21) | copy-start | bytes 393220
  97.3 28.9 %copy-start.12 = (f32[2048]{0:T(1024)S(1)}, f32[2048]{0:T(1024)}, u32[]{:S(2)}) copy-start(f32[2048]{0:T(1024)} %param.33) | copy-start | bytes 24580
  100.2 172.6 %reduce-scatter.8.cloned.1.call-start = ((), (), s32[]{:S(2)}) async-start(), calls=%async_computation.8 | async-start | bytes 3932160 | tf_op jit(solution)/shard_map/reduce_scatter | solution.py:249
  141.8 78.0 %copy-start.15 = (bf16[1,2048,512]{2,1,0:T(8,128)(2,1)S(1)}, bf16[1,2048,512]{2,1,0:T(8,128)(2,1)}, u32[]{:S(2)}) copy-start(bf16[1,2048,512]{2,1,0:T(8,128)(2,1)} %param.36) | copy-start | bytes 6291460
  218.0 1.7 copy-start.1
  272.8 25.6 %all-to-all-start.1 = ((bf16[8,1,96,512]{3,2,1,0:T(8,128)(2,1)}), bf16[8,1,96,512]{3,2,1,0:T(8,128)(2,1)S(1)}, u32[]{:S(2)}, u32[]{:S(2)}) async-start(bf16[8,1,96,512]{3,2,1,0:T(8,128)(2,1)} %bitcast.307), calls=%async_computation.4 | async-start | bytes 1572864 | tf_op jit(solution)/shard_map/all_to_all | solution.py:252
  277.4 36.7 %reduce-scatter.6.cloned.1.call-start = ((), (), s32[]{:S(2)}) async-start(), calls=%async_computation.7 | async-start | bytes 655360 | tf_op jit(solution)/shard_map/reduce_scatter | solution.py:266
  280.3 5.0 %copy-start.13 = (f32[128,4]{0,1:T(4,128)S(1)}, f32[128,4]{0,1:T(4,128)}, u32[]{:S(2)}) copy-start(f32[128,4]{0,1:T(4,128)} %param.35) | copy-start | bytes 6148
  303.3 10.9 %copy-start.3 = (bf16[32,2048]{1,0:T(8,128)(2,1)S(1)}, bf16[32,2048]{1,0:T(8,128)(2,1)}, u32[]{:S(2)}) copy-start(bf16[32,2048]{1,0:T(8,128)(2,1)} %reduce-scatter.4.cloned.1.call-done) | copy-start | bytes 393220
Sparse Core Ops, SparseCore 0:
  48.7 21.4 all-gather.8
  71.9 21.8 all-gather.6
  100.3 24.6 reduce-scatter.3
  230.9 41.8 reduce-scatter.7
  284.4 25.5 reduce-scatter.5
where the time goes:
time: 323 us; the launch traced here: 322 us
  blocking collectives  118 us (37%)
  waiting for transfers between devices  105 us (33%)
  matrix products  35.8 us (11%)
  local copies, waits for them, and re-layouts  24.5 us (8%)
  other arithmetic  16.2 us (5%)
  between operations  13.7 us (4%)
  starting transfers between devices  8.66 us (3%)
    all_to_all x1, blocking collectives, on_device(): lax.all_to_all(outgoing, 'sp', split_axis=0, concat_axis=0, tiled=True)  76.2 us
    reduce_scatter x1, waiting for transfers between devices, on_device(): lax.psum_scatter(partial_value.astype(jnp.bfloat16), 'tp', scatter_dimens...  42 us
    reduce_scatter x1, waiting for transfers between devices, on_device(): lax.psum_scatter(rounded(jnp.dot(picked_rows, mixer_output_weight, prefer...  20.8 us
    all_gather x1, waiting for transfers between devices, on_device(): lax.all_gather(forward_end[None].astype(jnp.bfloat16), 'sp', axis=0, tile...  20.5 us
    all_gather x1, blocking collectives, on_device(): lax.all_gather(backward_total[None].astype(jnp.bfloat16), 'sp', axis=0, t...  15.3 us
    all_to_all x1, waiting for transfers between devices, on_device(): lax.all_to_all(summed.astype(jnp.bfloat16), 'sp', split_axis=0, concat_ax...  12.4 us
    all_gather x1, blocking collectives, on_device(): all_rows = lax.all_gather(normed, 'tp', axis=0, tiled=True)  10.3 us
    all_gather x1, waiting for transfers between devices, on_device(): lax.all_gather(backward_end[None].astype(jnp.bfloat16), 'sp', axis=0, til...  9.52 us
  transfers between devices with their start and end apart: 8, of which 5 were waited for; matrix products, arithmetic and copies ran while one was open for 13% of the time, Pallas kernels for 0%

commit v1 on v0

v1 whole, which is shorter than its diff:
```python
import functools

import jax
import jax.numpy as jnp
from jax import lax
from jax.experimental import pallas as pl
from jax.experimental.pallas import tpu as pltpu
from jax.sharding import PartitionSpec as P

HD = 64
EPSILON = 1e-06
HIGHEST = lax.Precision.HIGHEST
MESH = pl.DeviceIdType.MESH
F32 = jnp.float32
BF16 = jnp.bfloat16
EDGE = 16


def exact_dot(a, b, contract):
    return lax.dot_general(
        a, b, (contract, ((), ())), precision=HIGHEST, preferred_element_type=F32
    )


def narrow_dot(a, b, contract=((1,), (0,))):
    return lax.dot_general(
        a.astype(BF16), b.astype(BF16), (contract, ((), ())), preferred_element_type=F32
    )


def mixer_kernel(
    n,
    parts,
    groups,
    joined_ref,
    taps_ref,
    pre_ref,
    spike_ref,
    bias_ref,
    rate_ref,
    gate_ref,
    gain_ref,
    wout_ref,
    resid_ref,
    fgain_ref,
    route_ref,
    resid_out,
    normed_out,
    route_out,
    halo,
    ends,
    got,
    part,
    part_got,
    halo_send,
    halo_recv,
    state_send,
    state_recv,
    part_send,
    part_recv,
    route_send,
    route_recv,
    local_sem,
):
    d = lax.axis_index("sp")
    me = lax.axis_index("tp")
    length, width = gate_ref.shape
    heads = width // HD
    total_cols = joined_ref.shape[1]
    states = (total_cols - width) // (2 * groups)
    taps = taps_ref.shape[0]
    margin = taps // 2
    rows = length // parts
    barrier = pltpu.get_barrier_semaphore()
    for k in range(1, n):
        pl.semaphore_signal(
            barrier, inc=1, device_id={"sp": lax.rem(d + k, n)}, device_id_type=MESH
        )
    for k in range(1, parts):
        pl.semaphore_signal(
            barrier, inc=1, device_id={"tp": lax.rem(me + k, parts)}, device_id_type=MESH
        )
    pl.semaphore_wait(barrier, n + parts - 2)

    down = pltpu.make_async_remote_copy(
        src_ref=joined_ref.at[pl.ds(length - EDGE, EDGE)],
        dst_ref=halo.at[0],
        send_sem=halo_send.at[0],
        recv_sem=halo_recv.at[0],
        device_id={"sp": lax.rem(d + 1, n)},
        device_id_type=MESH,
    )
    up = pltpu.make_async_remote_copy(
        src_ref=joined_ref.at[pl.ds(0, EDGE)],
        dst_ref=halo.at[1],
        send_sem=halo_send.at[1],
        recv_sem=halo_recv.at[1],
        device_id={"sp": lax.rem(d + n - 1, n)},
        device_id_type=MESH,
    )
    down.start()
    up.start()
    route_copies = []
    for k in range(1, n):
        copy = pltpu.make_async_remote_copy(
            src_ref=route_ref,
            dst_ref=route_out.at[d],
            send_sem=route_send.at[k - 1],
            recv_sem=route_recv.at[k - 1],
            device_id={"sp": lax.rem(d + k, n)},
            device_id_type=MESH,
        )
        copy.start()
        route_copies.append(copy)
    own_route = pltpu.make_async_copy(route_ref, route_out.at[d], local_sem)
    own_route.start()

    pre = pre_ref[...] + bias_ref[...]
    step = jnp.maximum(pre, 0.0) + jnp.log1p(jnp.exp(-jnp.abs(pre)))
    decay = spike_ref[...] - step * jnp.exp(rate_ref[...])
    row_i = lax.broadcasted_iota(jnp.int32, (length, length), 0)
    col_i = lax.broadcasted_iota(jnp.int32, (length, length), 1)
    upto = jnp.where(row_i >= col_i, 1.0, 0.0).astype(F32)
    ones = jnp.ones((8, length), F32)
    eye = jnp.where(row_i == col_i, 1.0, 0.0).astype(F32)
    within = exact_dot(upto, decay, ((1,), (0,)))
    before = within - decay
    total = exact_dot(ones, decay, ((1,), (0,)))[0:1]
    within_t = exact_dot(within, eye, ((0,), (0,)))
    before_t = exact_dot(before, eye, ((0,), (0,)))
    step_t = exact_dot(step, eye, ((0,), (0,)))
    spread_head = lax.broadcasted_iota(jnp.int32, (heads, width), 0)
    spread_col = lax.broadcasted_iota(jnp.int32, (heads, width), 1)
    spread = jnp.where(spread_col // HD == spread_head, 1.0, 0.0).astype(F32)

    def widen(cells):
        return exact_dot(cells, spread, ((1,), (0,)))

    wf, ef = within[:, :heads], before[:, heads:]
    tf, tb = total[:, :heads], total[:, heads:]
    tail_f = widen(step[:, :heads] * jnp.exp(tf - wf))
    tail_b = widen(step[:, heads:] * jnp.exp(ef))
    head_f = widen(jnp.exp(wf))
    head_b = widen(jnp.exp(tb - ef))
    eight = jnp.zeros((8, heads), F32)
    total_f = widen(eight + tf)[0:1]
    total_b = widen(eight + tb)[0:1]

    down.wait()
    up.wait()
    previous = jnp.where(d > 0, halo[0].astype(F32), 0.0)
    following = jnp.where(d < n - 1, halo[1].astype(F32), 0.0)
    padded = jnp.concatenate([previous, joined_ref[...].astype(F32), following], axis=0)
    extent = length + 2 * EDGE
    conv = jnp.zeros((length, total_cols), F32)
    for k in range(taps):
        shift = (margin - k) % extent
        moved = pltpu.roll(padded, shift, 0) if shift else padded
        conv = conv + taps_ref[k : k + 1, :] * moved[EDGE : EDGE + length]
    act = conv * jax.nn.sigmoid(conv)
    values = act[:, :width]
    bs = [act[:, width + g * states : width + (g + 1) * states].astype(BF16) for g in range(groups)]
    cs = [
        act[:, width + (groups + g) * states : width + (groups + g + 1) * states].astype(BF16)
        for g in range(groups)
    ]
    share = width // groups
    end_row = lax.broadcasted_iota(jnp.int32, (EDGE, width), 0)
    for way, tail, tot in ((0, tail_f, total_f), (1, tail_b, total_b)):
        weighted = (values * tail).astype(BF16)
        for g in range(groups):
            cols = slice(g * share, (g + 1) * share)
            ends[way, 0:states, cols] = narrow_dot(bs[g], weighted[:, cols], ((0,), (0,))).astype(
                BF16
            )
        high = tot.astype(BF16).astype(F32)
        low = tot - high
        ends[way, states : states + EDGE, :] = jnp.where(
            end_row == 0, high, jnp.where(end_row == 1, low, 0.0)
        ).astype(BF16)
    state_copies = []
    for k in range(1, n):
        copy = pltpu.make_async_remote_copy(
            src_ref=ends.at[(d + k) // n],
            dst_ref=got.at[k - 1],
            send_sem=state_send.at[k - 1],
            recv_sem=state_recv.at[k - 1],
            device_id={"sp": lax.rem(d + k, n)},
            device_id_type=MESH,
        )
        copy.start()
        state_copies.append(copy)

    blocks = []
    heads_in = heads // groups
    for g in range(groups):
        scores = narrow_dot(cs[g], bs[g], ((1,), (1,)))
        for h in range(g * heads_in, (g + 1) * heads_in):
            b = heads + h
            spread_f = within[:, h : h + 1] - within_t[h : h + 1, :]
            spread_b = before_t[b : b + 1, :] - before[:, b : b + 1]
            factor = jnp.exp(jnp.where(row_i >= col_i, spread_f, spread_b))
            sf, sb = step_t[h : h + 1, :], step_t[b : b + 1, :]
            coeff = jnp.where(row_i >= col_i, sf, 0.0) + jnp.where(row_i <= col_i, sb, 0.0)
            mat = (scores * factor * coeff).astype(BF16)
            blocks.append(narrow_dot(mat, values[:, h * HD : (h + 1) * HD]))
    out = jnp.concatenate(blocks, axis=1)
    gate = gate_ref[...].astype(F32)
    gate = gate * jax.nn.sigmoid(gate)

    for copy in state_copies:
        copy.wait()
    weight = jnp.where(d >= 1, 1.0, 0.0) * jnp.ones((1, width), F32)
    start_f = jnp.zeros((states, width), F32)
    for k in range(1, n):
        weight = jnp.where(d >= k, weight, 0.0)
        start_f = start_f + weight * got[k - 1, 0:states, :].astype(F32)
        marks = got[k - 1, states : states + EDGE, :].astype(F32)
        weight = weight * jnp.exp(marks[0:1] + marks[1:2])
    weight = jnp.ones((1, width), F32)
    start_b = jnp.zeros((states, width), F32)
    for m in range(1, n):
        weight = jnp.where(d + m < n, weight, 0.0)
        slot = n - m - 1
        start_b = start_b + weight * got[slot, 0:states, :].astype(F32)
        marks = got[slot, states : states + EDGE, :].astype(F32)
        weight = weight * jnp.exp(jnp.minimum(marks[0:1] + marks[1:2], 0.0))
    carried = []
    for g in range(groups):
        cols = slice(g * share, (g + 1) * share)
        carried.append(
            head_f[:, cols] * narrow_dot(cs[g], start_f[:, cols])
            + head_b[:, cols] * narrow_dot(cs[g], start_b[:, cols])
        )
    out = out + (carried[0] if groups == 1 else jnp.concatenate(carried, axis=1))
    gated = out * gate
    square = exact_dot(gated * gated, spread, ((1,), (1,))) * (1.0 / HD)
    scale = widen(lax.rsqrt(square + EPSILON))
    mixed = (gated * scale * gain_ref[...]).astype(BF16)
    model = wout_ref.shape[1]
    tile = min(512, model)
    for c in range(0, model, tile):
        part[:, c : c + tile] = jnp.dot(
            mixed, wout_ref[:, c : c + tile], preferred_element_type=F32
        ).astype(BF16)
    part_copies = []
    for k in range(1, parts):
        target = lax.rem(me + k, parts)
        copy = pltpu.make_async_remote_copy(
            src_ref=part.at[pl.ds(pl.multiple_of(target * rows, rows), rows)],
            dst_ref=part_got.at[k - 1],
            send_sem=part_send.at[k - 1],
            recv_sem=part_recv.at[k - 1],
            device_id={"tp": target},
            device_id_type=MESH,
        )
        copy.start()
        part_copies.append(copy)
    residual = resid_ref[...].astype(F32) + part[
        pl.ds(pl.multiple_of(me * rows, rows), rows), :
    ].astype(F32)
    for k in range(1, parts):
        part_copies[k - 1].wait()
        residual = residual + part_got[k - 1].astype(F32)
    residual = residual.astype(BF16)
    resid_out[...] = residual
    wide = residual.astype(F32)
    mean = jnp.mean(wide * wide, axis=1, keepdims=True)
    normed_out[...] = (wide * lax.rsqrt(mean + EPSILON) * fgain_ref[...]).astype(BF16)
    own_route.wait()
    for copy in route_copies:
        copy.wait()


def on_device(
    residual_input,
    mixer_value_input,
    gate_preactivation,
    state_projection_input,
    step_preactivation,
    spike_log_decay,
    value_filter_taps,
    state_projection_taps,
    step_size_bias,
    head_log_decay,
    gated_norm_gain,
    mixer_output_weight,
    feedforward_norm_gain,
    routed_expert_index,
    routed_expert_weight,
    routed_gate_weight,
    routed_up_weight,
    routed_down_weight,
    common_gate_weight,
    common_up_weight,
    common_down_weight,
):
    n, parts = (lax.axis_size("sp"), lax.axis_size("tp"))
    seq_rows, width = mixer_value_input.shape
    heads = width // HD
    all_groups, states = state_projection_input.shape[2:]
    per_group = heads * parts // all_groups
    groups = max(1, heads // per_group)
    first_group = lax.axis_index("tp") * heads // per_group
    taps = value_filter_taps.shape[0]
    model = mixer_output_weight.shape[1]
    rows = residual_input.shape[0]
    local_experts = routed_gate_weight.shape[0]
    experts = local_experts * n
    bc = lax.dynamic_slice_in_dim(state_projection_input, first_group, groups, 2)
    bc_taps = lax.dynamic_slice_in_dim(state_projection_taps, first_group, groups, 2)
    joined = jnp.concatenate(
        [mixer_value_input, bc.reshape(seq_rows, 2 * groups * states)], axis=1
    )
    kernel = jnp.concatenate(
        [value_filter_taps, bc_taps.reshape(taps, 2 * groups * states)], axis=1
    )
    named = routed_expert_index[None] == jnp.arange(experts, dtype=jnp.int32)[:, None, None]
    route = jnp.sum(jnp.where(named, routed_expert_weight[None], 0.0), axis=2)
    cols = joined.shape[1]
    vmem = pl.BlockSpec(memory_space=pltpu.VMEM)
    dma = pltpu.SemaphoreType.DMA
    residual, normed, routes = pl.pallas_call(
        functools.partial(mixer_kernel, n, parts, groups),
        out_shape=(
            jax.ShapeDtypeStruct((rows, model), BF16),
            jax.ShapeDtypeStruct((rows, model), BF16),
            jax.ShapeDtypeStruct((n, experts, seq_rows), F32),
        ),
        in_specs=[vmem] * 12,
        out_specs=(vmem, vmem, vmem),
        scratch_shapes=[
            pltpu.VMEM((2, EDGE, cols), BF16),
            pltpu.VMEM((2, states + EDGE, width), BF16),
            pltpu.VMEM((n - 1, states + EDGE, width), BF16),
            pltpu.VMEM((seq_rows, model), BF16),
            pltpu.VMEM((parts - 1, rows, model), BF16),
            dma((2,)),
            dma((2,)),
            dma((n - 1,)),
            dma((n - 1,)),
            dma((parts - 1,)),
            dma((parts - 1,)),
            dma((n - 1,)),
            dma((n - 1,)),
            dma,
        ],
        compiler_params=pltpu.CompilerParams(collective_id=0, has_side_effects=True),
        name="mixer",
    )(
        joined,
        kernel,
        step_preactivation.astype(F32).reshape(seq_rows, 2 * heads),
        spike_log_decay.reshape(seq_rows, 2 * heads),
        step_size_bias.reshape(1, 2 * heads),
        head_log_decay.reshape(1, 2 * heads),
        gate_preactivation,
        gated_norm_gain.reshape(1, width),
        mixer_output_weight,
        residual_input,
        feedforward_norm_gain.reshape(1, model),
        route,
    )
    d = lax.axis_index("sp")
    every = lax.all_gather(normed, ("sp", "tp"), axis=0, tiled=True)
    mine = lax.dynamic_slice_in_dim(every, d * seq_rows, seq_rows, 0)

    def ffn(x, wg, wu, wd, scale):
        gate = jnp.dot(x, wg, preferred_element_type=F32)
        up = jnp.dot(x, wu, preferred_element_type=F32)
        hidden = jax.nn.silu(gate) * up
        if scale is not None:
            hidden = hidden * scale
        return jnp.dot(hidden.astype(BF16), wd, preferred_element_type=F32)

    shared = ffn(mine, common_gate_weight, common_up_weight, common_down_weight, None)
    here = (jnp.arange(n, dtype=jnp.int32) == d)[:, None, None]
    partial = jnp.where(here, shared[None], 0.0)
    for e in range(local_experts):
        scale = lax.dynamic_index_in_dim(routes, d * local_experts + e, 1, keepdims=False)
        partial = partial + ffn(
            every,
            routed_gate_weight[e],
            routed_up_weight[e],
            routed_down_weight[e],
            scale.reshape(n * seq_rows, 1),
        ).reshape(n, seq_rows, model)
    feed = lax.psum_scatter(
        partial.astype(BF16).reshape(n * seq_rows, model),
        ("sp", "tp"),
        scatter_dimension=0,
        tiled=True,
    )
    return (residual.astype(F32) + feed.astype(F32)).astype(BF16)


def solution(mesh):
    return jax.shard_map(
        on_device,
        mesh=mesh,
        in_specs=(
            P(("sp", "tp"), None),
            P("sp", "tp"),
            P("sp", "tp"),
            P("sp", None, None, None),
            P("sp", None, "tp"),
            P("sp", None, "tp"),
            P(None, "tp"),
            P(),
            P(None, "tp"),
            P(None, "tp"),
            P("tp"),
            P("tp", None),
            P(),
            P("sp", None),
            P("sp", None),
            P("sp", None, "tp"),
            P("sp", None, "tp"),
            P("sp", "tp", None),
            P(None, "tp"),
            P(None, "tp"),
            P("tp", None),
        ),
        out_specs=P(("sp", "tp"), None),
        check_vma=False,
    )
```

time: 323 us -> 296 us (0.916)
  blocking collectives: 118 us -> 0 us
  waiting for transfers between devices: 105 us -> 208 us
  Pallas kernels: 0 us -> 40.8 us
  matrix products: 35.8 us -> 18.3 us
  local copies, waits for them, and re-layouts: 24.5 us -> 8.95 us
  other arithmetic: 16.2 us -> 6.49 us
  starting transfers between devices: 8.66 us -> 0.04 us
    all_to_all x2 -> x0, blocking collectives: 83.8 us -> none  [the longest x1 76.2 us: on_device(): lax.all_to_all(outgoing, 'sp', split_axis=0, concat_axis=0, tiled=True)]
    reduce_scatter x3 -> x1, waiting for transfers between devices: 62.8 us -> 142 us  [on_device(): lax.psum_scatter(partial.astype(BF16).reshape(n * seq_rows, model), ('sp'...]
    pallas_call x0 -> x1, Pallas kernels: none -> 40.8 us  [on_device(): pl.pallas_call(functools.partial(mixer_kernel, n, parts, groups), out_sha...]
    all_gather x2 -> x1, waiting for transfers between devices: 30 us -> 65.6 us  [on_device(): every = lax.all_gather(normed, ('sp', 'tp'), axis=0, tiled=True)]
    all_gather x3 -> x0, blocking collectives: 34.3 us -> none  [the longest x1 15.3 us: on_device(): lax.all_gather(backward_total[None].astype(jnp.bfloat16), 'sp', axis=0, t...]
    dot_general x17 -> x5, matrix products: 35.8 us -> 18.3 us  [the longest x2 8.81 us: ffn(): return jnp.dot(hidden.astype(BF16), wd, preferred_element_type=F32)]
    all_to_all x1 -> x0, waiting for transfers between devices: 12.4 us -> none  [on_device(): lax.all_to_all(summed.astype(jnp.bfloat16), 'sp', split_axis=0, concat_ax...]
    gather x3 -> x0, local copies, waits for them, and re-layouts: 9 us -> none  [the longest x2 4.73 us: on_device(): chosen = flat_back[slot_index]]
  transfers between devices with their start and end apart: 8 -> 2, of which waited for: 5 -> 2; matrix products, arithmetic and copies ran while one was open for 13% -> 0% of each run, Pallas kernels for 0% -> 0%
where the time goes in v1:
time: 296 us
  waiting for transfers between devices  208 us (70%)
  Pallas kernels  40.8 us (14%)
  matrix products  18.3 us (6%)
  between operations  13.5 us (5%)
  local copies, waits for them, and re-layouts  8.95 us (3%)
  other arithmetic  6.49 us (2%)
    reduce_scatter x1, waiting for transfers between devices, on_device(): lax.psum_scatter(partial.astype(BF16).reshape(n * seq_rows, model), ('sp'...  142 us
    all_gather x1, waiting for transfers between devices, on_device(): every = lax.all_gather(normed, ('sp', 'tp'), axis=0, tiled=True)  65.6 us
    pallas_call x1, Pallas kernels, on_device(): pl.pallas_call(functools.partial(mixer_kernel, n, parts, groups), out_sha...  40.8 us
    dot_general x2, matrix products, ffn(): return jnp.dot(hidden.astype(BF16), wd, preferred_element_type=F32)  8.81 us
  transfers between devices with their start and end apart: 2, of which 2 were waited for; matrix products, arithmetic and copies ran while one was open for 0% of the time, Pallas kernels for 0%

profile of v1, /device:TPU:0, one launch (start us, length us, event | category | flops | bytes accessed | tf_op | source)
XLA Modules:
  0.0 295.6 jit_solution(2962996707708431397)
XLA Ops:
  6.5 0.0 copy-start
  6.5 0.0 all-gather.2.cloned.1.call-start
  6.5 1.2 constant_dynamic-slice_fusion.1
  7.8 0.1 copy.36
  7.9 0.1 copy.33
  8.0 0.8 dynamic-slice_reduce_fusion
  8.8 0.7 bitcast_convert_fusion
  9.5 0.7 copy.34.pre_ref
  10.2 1.4 copy.35.spike_ref
  11.6 1.3 reshape.46.bias_ref
  13.0 1.3 reshape.47.rate_ref
  14.3 1.6 pad_maximum_fusion.joined_ref
  15.9 1.3 pad_maximum_fusion.1.taps_ref
  17.2 1.3 select_reduce_fusion.route_ref
  18.5 40.8 %mixer.1 = (bf16[32,2048]{1,0:T(8,128)(2,1)}, bf16[32,2048]{1,0:T(8,128)(2,1)}, f32[8,8,128]{2,1,0:T(8,128)}) custom-call(bf16[128,768]{1,0:T(8,128)(2,1)} %pad_maximum_fusion.joined_ref, f32[5,768]{1,0:T(8,128)} %pad_maximum_fusion.1.taps_ref, f32[128,16]{1,0:T(8,128)} %copy.34.pre_ref, f32[128,16]{1,0:T(8,128)} %copy.35.spike_ref, ...), custom_call_target="tpu_custom_call" | custom-call | tf_op jit(solution)/shard_map/mixer/pallas_call | solution.py:323
  59.3 0.0 all-gather.2.cloned.1.call-update
  59.3 0.0 reduce-scatter.2.cloned.1.call-start
  59.4 0.8 constant_dynamic-slice_fusion
  60.1 65.6 %all-gather.2.cloned.1.call-done = bf16[1024,2048]{1,0:T(8,128)(2,1)} async-done(((bf16[32,2048]{1,0:T(8,128)(2,1)}), bf16[1024,2048]{1,0:T(8,128)(2,1)}) %all-gather.2.cloned.1.call-update) | async-done | bytes 4194320 | tf_op jit(solution)/shard_map/all_gather | solution.py:365
  125.8 0.0 copy-start.1
  125.8 0.0 copy-start.2
  125.8 5.3 %fusion.1 = f32[1024,512]{1,0:T(8,128)S(1)} fusion(bf16[1024,2048]{1,0:T(8,128)(2,1)} %all-gather.2.cloned.1.call-done, bf16[1,2048,512]{2,1,0:T(8,128)(2,1)} %param.37), kind=kOutput, calls=%fused_computation.2 | convolution fusion | flops 2147483648 | bytes 8388608 | tf_op jit(solution)/shard_map/dot_general | solution.py:370
  131.1 0.0 copy-done.1
  131.1 0.0 copy-done.2
  131.1 0.0 copy-start.4
  131.1 0.5 fusion.11
  131.6 1.1 copy-done.4
  132.7 3.7 %multiply_convert_fusion = bf16[1024,512]{1,0:T(8,128)(2,1)} fusion(f32[1024,512]{1,0:T(8,128)S(1)} %fusion.1, bf16[1024,2048]{1,0:T(8,128)(2,1)S(1)} %copy-done.2, bf16[1,2048,512]{2,1,0:T(8,128)(2,1)S(1)} %copy-done.4, f32[1024]{0:T(1024)S(1)} %bitcast.38), kind=kOutput, calls=%fused_computation.6 | convolution fusion | flops 2151153664 | bytes 9441280 | tf_op jit(solution)/shard_map/dot_general | solution.py:369
  136.4 3.2 %fusion.8 = f32[128,2048]{1,0:T(8,128)S(1)} fusion(bf16[512,2048]{1,0:T(8,128)(2,1)} %param.41, bf16[2048,512]{1,0:T(8,128)(2,1)} %param.40, bf16[1024,2048]{1,0:T(8,128)(2,1)} %all-gather.2.cloned.1.call-done, s32[]{:T(128)S(6)} %select_n.27, f32[128,512]{1,0:T(8,128)S(1)} %fusion.11), kind=kOutput, calls=%fused_computation.9 | convolution fusion | flops 537264128 | bytes 6029316 | tf_op jit(solution)/shard_map/dot_general | solution.py:374
  139.6 0.0 copy-done
  139.6 5.6 %add_convert_fusion = bf16[8,128,2048]{2,1,0:T(8,128)(2,1)} fusion(f32[128,2048]{1,0:T(8,128)S(1)} %fusion.8, pred[8]{0:T(512)(128)(4,1)S(1)} %iota_compare_fusion.1, bf16[8,128,512]{2,1,0:T(8,128)(2,1)} %bitcast.40, bf16[1,512,2048]{2,1,0:T(8,128)(2,1)S(1)} %copy-done), kind=kOutput, calls=%fused_computation | convolution fusion | flops 2153775104 | bytes 8388616 | tf_op jit(solution)/shard_map/dot_general | solution.py:374
  145.2 0.0 copy-start.3
  145.2 0.0 reduce-scatter.2.cloned.1.call-update
  145.2 142.0 %reduce-scatter.2.cloned.1.call-done = bf16[32,2048]{1,0:T(8,128)(2,1)} async-done(((bf16[1024,2048]{1,0:T(8,128)(2,1)}), bf16[32,2048]{1,0:T(8,128)(2,1)}) %reduce-scatter.2.cloned.1.call-update) | async-done | bytes 131088 | tf_op jit(solution)/shard_map/reduce_scatter | solution.py:388
  287.2 0.0 copy-done.3
  287.2 1.6 add_convert_fusion.1
  (2 shorter events, 0.0 us)
Async XLA Ops:
  6.5 133.1 %copy-start = (bf16[1,512,2048]{2,1,0:T(8,128)(2,1)S(1)}, bf16[1,512,2048]{2,1,0:T(8,128)(2,1)}, u32[]{:S(2)}) copy-start(bf16[1,512,2048]{2,1,0:T(8,128)(2,1)} %param.38) | copy-start | bytes 6291460
  6.5 119.2 %all-gather.2.cloned.1.call-start = ((), (), s32[]{:S(2)}) async-start(), calls=%async_computation.1 | async-start | bytes 4325376 | tf_op jit(solution)/shard_map/all_gather | solution.py:365
  59.3 227.9 %reduce-scatter.2.cloned.1.call-start = ((), (), s32[]{:S(2)}) async-start(), calls=%async_computation.2 | async-start | bytes 4325376 | tf_op jit(solution)/shard_map/reduce_scatter | solution.py:388
  125.8 5.3 %copy-start.1 = (bf16[2048,512]{1,0:T(8,128)(2,1)S(1)}, bf16[2048,512]{1,0:T(8,128)(2,1)}, u32[]{:S(2)}) copy-start(bf16[2048,512]{1,0:T(8,128)(2,1)} %param.39) | copy-start | bytes 6291460
  125.8 5.3 %copy-start.2 = (bf16[1024,2048]{1,0:T(8,128)(2,1)S(1)}, bf16[1024,2048]{1,0:T(8,128)(2,1)}, u32[]{:S(2)}) copy-start(bf16[1024,2048]{1,0:T(8,128)(2,1)} %all-gather.2.cloned.1.call-done) | copy-start | bytes 12582916
  131.1 1.6 copy-start.4
  145.2 142.0 %copy-start.3 = (bf16[32,2048]{1,0:T(8,128)(2,1)S(1)}, bf16[32,2048]{1,0:T(8,128)(2,1)}, u32[]{:S(2)}) copy-start(bf16[32,2048]{1,0:T(8,128)(2,1)} %get-tuple-element.8) | copy-start | bytes 393220
Sparse Core Ops, SparseCore 0:
  59.4 66.2 all-gather.1
  145.4 141.8 reduce-scatter.1

commit v2 on v1

--- a/solution.py
+++ b/solution.py
@@ -33,7 +33,8 @@
     parts,
     groups,
     joined_ref,
-    taps_ref,
+    value_taps_ref,
+    state_taps_ref,
     pre_ref,
     spike_ref,
     bias_ref,
@@ -68,7 +69,7 @@
     heads = width // HD
     total_cols = joined_ref.shape[1]
     states = (total_cols - width) // (2 * groups)
-    taps = taps_ref.shape[0]
+    taps = value_taps_ref.shape[0]
     margin = taps // 2
     rows = length // parts
     barrier = pltpu.get_barrier_semaphore()
@@ -115,9 +116,11 @@
     own_route = pltpu.make_async_copy(route_ref, route_out.at[d], local_sem)
     own_route.start()
 
-    pre = pre_ref[...] + bias_ref[...]
+    bias = jnp.concatenate([bias_ref[0:1, :], bias_ref[1:2, :]], axis=1)
+    rate = jnp.concatenate([rate_ref[0:1, :], rate_ref[1:2, :]], axis=1)
+    pre = pre_ref[...] + bias
     step = jnp.maximum(pre, 0.0) + jnp.log1p(jnp.exp(-jnp.abs(pre)))
-    decay = spike_ref[...] - step * jnp.exp(rate_ref[...])
+    decay = spike_ref[...] - step * jnp.exp(rate)
     row_i = lax.broadcasted_iota(jnp.int32, (length, length), 0)
     col_i = lax.broadcasted_iota(jnp.int32, (length, length), 1)
     upto = jnp.where(row_i >= col_i, 1.0, 0.0).astype(F32)
@@ -152,11 +155,12 @@
     following = jnp.where(d < n - 1, halo[1].astype(F32), 0.0)
     padded = jnp.concatenate([previous, joined_ref[...].astype(F32), following], axis=0)
     extent = length + 2 * EDGE
+    filters = jnp.concatenate([value_taps_ref[...], state_taps_ref[...]], axis=1)
     conv = jnp.zeros((length, total_cols), F32)
     for k in range(taps):
         shift = (margin - k) % extent
         moved = pltpu.roll(padded, shift, 0) if shift else padded
-        conv = conv + taps_ref[k : k + 1, :] * moved[EDGE : EDGE + length]
+        conv = conv + filters[k : k + 1, :] * moved[EDGE : EDGE + length]
     act = conv * jax.nn.sigmoid(conv)
     values = act[:, :width]
     bs = [act[:, width + g * states : width + (g + 1) * states].astype(BF16) for g in range(groups)]
@@ -270,6 +274,169 @@
     own_route.wait()
     for copy in route_copies:
         copy.wait()
+
+
+def remote(src, dst, send, recv, where):
+    return pltpu.make_async_remote_copy(
+        src_ref=src,
+        dst_ref=dst,
+        send_sem=send,
+        recv_sem=recv,
+        device_id=where,
+        device_id_type=MESH,
+    )
+
+
+def greet(n, parts, d, me, other):
+    barrier = pltpu.get_barrier_semaphore()
+    for k in range(1, n // 2):
+        pl.semaphore_signal(
+            barrier, inc=1, device_id={"sp": lax.rem(d + 2 * k, n)}, device_id_type=MESH
+        )
+    for k in range(1, parts):
+        pl.semaphore_signal(
+            barrier, inc=1, device_id={"tp": lax.rem(me + k, parts)}, device_id_type=MESH
+        )
+    pl.semaphore_signal(barrier, inc=1, device_id={"sp": other}, device_id_type=MESH)
+    pl.semaphore_wait(barrier, n // 2 + parts - 1)
+
+
+def gather_kernel(n, parts, x_ref, out, zs, zr, ts, tr, cs, cr, local_sem):
+    d, me = lax.axis_index("sp"), lax.axis_index("tp")
+    other = d + 1 - 2 * lax.rem(d, 2)
+    chips = n // 2
+    greet(n, parts, d, me, other)
+    z_copies = [None]
+    for k in range(1, chips):
+        copy = remote(
+            x_ref,
+            out.at[d, me],
+            zs.at[k - 1],
+            zr.at[k - 1],
+            {"sp": lax.rem(d + 2 * k, n)},
+        )
+        copy.start()
+        z_copies.append(copy)
+    own = pltpu.make_async_copy(x_ref, out.at[d, me], local_sem)
+    own.start()
+    t_copies = []
+    for j in range(chips):
+        block = lax.rem(d + n - 2 * j, n)
+        if j:
+            z_copies[j].wait_recv()
+        row = []
+        for k in range(1, parts):
+            copy = remote(
+                out.at[block, me] if j else x_ref,
+                out.at[block, me],
+                ts.at[j, k - 1],
+                tr.at[j, k - 1],
+                {"tp": lax.rem(me + k, parts)},
+            )
+            copy.start()
+            row.append(copy)
+        t_copies.append(row)
+    own.wait()
+    c_copies = []
+    for j in range(chips):
+        block = lax.rem(d + n - 2 * j, n)
+        for copy in t_copies[j]:
+            copy.wait_recv()
+        copy = remote(out.at[block], out.at[block], cs.at[j], cr.at[j], {"sp": other})
+        copy.start()
+        c_copies.append(copy)
+    for copy in z_copies[1:]:
+        copy.wait_send()
+    for row in t_copies:
+        for copy in row:
+            copy.wait_send()
+    for copy in c_copies:
+        copy.wait()
+
+
+def sum_kernel(
+    n,
+    parts,
+    x_ref,
+    resid_ref,
+    out_ref,
+    c_got,
+    paired,
+    t_got,
+    ready,
+    z_got,
+    zs,
+    zr,
+    ts,
+    tr,
+    cs,
+    cr,
+):
+    d, me = lax.axis_index("sp"), lax.axis_index("tp")
+    core = lax.rem(d, 2)
+    z = d // 2
+    other = d + 1 - 2 * core
+    chips = n // 2
+    greet(n, parts, d, me, other)
+    order = list(range(1, chips)) + [0]
+    c_copies = {}
+    for k in order:
+        chip = lax.rem(z + k, chips)
+        copy = remote(
+            x_ref.at[2 * chip + 1 - core], c_got.at[k], cs.at[k], cr.at[k], {"sp": other}
+        )
+        copy.start()
+        c_copies[k] = copy
+    t_copies = {}
+    for k in order:
+        chip = lax.rem(z + k, chips)
+        c_copies[k].wait_recv()
+
+        def add(t, carry, k=k, chip=chip):
+            paired[k, t] = (
+                x_ref[2 * chip + core, t].astype(F32) + c_got[k, t].astype(F32)
+            ).astype(BF16)
+            return carry
+
+        lax.fori_loop(0, parts, add, 0)
+        for q in range(1, parts):
+            t = lax.rem(me + q, parts)
+            copy = remote(
+                paired.at[k, t],
+                t_got.at[k, q - 1],
+                ts.at[k, q - 1],
+                tr.at[k, q - 1],
+                {"tp": t},
+            )
+            copy.start()
+            t_copies[k, q] = copy
+    z_copies = {}
+    for k in order:
+        total = paired[k, me].astype(F32)
+        for q in range(1, parts):
+            t_copies[k, q].wait_recv()
+            total = total + t_got[k, q - 1].astype(F32)
+        if k:
+            ready[k - 1] = total.astype(BF16)
+            copy = remote(
+                ready.at[k - 1],
+                z_got.at[k - 1],
+                zs.at[k - 1],
+                zr.at[k - 1],
+                {"sp": lax.rem(d + 2 * k, n)},
+            )
+            copy.start()
+            z_copies[k] = copy
+    for k in range(1, chips):
+        z_copies[k].wait_recv()
+        total = total + z_got[k - 1].astype(F32)
+    out_ref[...] = (resid_ref[...].astype(F32) + total).astype(BF16)
+    for copy in c_copies.values():
+        copy.wait_send()
+    for copy in t_copies.values():
+        copy.wait_send()
+    for copy in z_copies.values():
+        copy.wait_send()
 
 
 def on_device(
@@ -312,9 +479,6 @@
     joined = jnp.concatenate(
         [mixer_value_input, bc.reshape(seq_rows, 2 * groups * states)], axis=1
     )
-    kernel = jnp.concatenate(
-        [value_filter_taps, bc_taps.reshape(taps, 2 * groups * states)], axis=1
-    )
     named = routed_expert_index[None] == jnp.arange(experts, dtype=jnp.int32)[:, None, None]
     route = jnp.sum(jnp.where(named, routed_expert_weight[None], 0.0), axis=2)
     cols = joined.shape[1]
@@ -327,7 +491,7 @@
             jax.ShapeDtypeStruct((rows, model), BF16),
             jax.ShapeDtypeStruct((n, experts, seq_rows), F32),
         ),
-        in_specs=[vmem] * 12,
+        in_specs=[vmem] * 13,
         out_specs=(vmem, vmem, vmem),
         scratch_shapes=[
             pltpu.VMEM((2, EDGE, cols), BF16),
@@ -349,11 +513,12 @@
         name="mixer",
     )(
         joined,
-        kernel,
+        value_filter_taps,
+        bc_taps.reshape(taps, 2 * groups * states),
         step_preactivation.astype(F32).reshape(seq_rows, 2 * heads),
         spike_log_decay.reshape(seq_rows, 2 * heads),
-        step_size_bias.reshape(1, 2 * heads),
-        head_log_decay.reshape(1, 2 * heads),
+        step_size_bias,
+        head_log_decay,
         gate_preactivation,
         gated_norm_gain.reshape(1, width),
         mixer_output_weight,
@@ -362,7 +527,24 @@
         route,
     )
     d = lax.axis_index("sp")
-    every = lax.all_gather(normed, ("sp", "tp"), axis=0, tiled=True)
+    chips = n // 2
+    every = pl.pallas_call(
+        functools.partial(gather_kernel, n, parts),
+        out_shape=jax.ShapeDtypeStruct((n, parts, rows, model), BF16),
+        in_specs=[vmem],
+        out_specs=vmem,
+        scratch_shapes=[
+            dma((chips - 1,)),
+            dma((chips - 1,)),
+            dma((chips, parts - 1)),
+            dma((chips, parts - 1)),
+            dma((chips,)),
+            dma((chips,)),
+            dma,
+        ],
+        compiler_params=pltpu.CompilerParams(collective_id=1, has_side_effects=True),
+        name="gather_rows",
+    )(normed).reshape(n * seq_rows, model)
     mine = lax.dynamic_slice_in_dim(every, d * seq_rows, seq_rows, 0)
 
     def ffn(x, wg, wu, wd, scale):
@@ -385,13 +567,27 @@
             routed_down_weight[e],
             scale.reshape(n * seq_rows, 1),
         ).reshape(n, seq_rows, model)
-    feed = lax.psum_scatter(
-        partial.astype(BF16).reshape(n * seq_rows, model),
-        ("sp", "tp"),
-        scatter_dimension=0,
-        tiled=True,
-    )
-    return (residual.astype(F32) + feed.astype(F32)).astype(BF16)
+    return pl.pallas_call(
+        functools.partial(sum_kernel, n, parts),
+        out_shape=jax.ShapeDtypeStruct((rows, model), BF16),
+        in_specs=[vmem, vmem],
+        out_specs=vmem,
+        scratch_shapes=[
+            pltpu.VMEM((chips, parts, rows, model), BF16),
+            pltpu.VMEM((chips, parts, rows, model), BF16),
+            pltpu.VMEM((chips, parts - 1, rows, model), BF16),
+            pltpu.VMEM((chips - 1, rows, model), BF16),
+            pltpu.VMEM((chips - 1, rows, model), BF16),
+            dma((chips - 1,)),
+            dma((chips - 1,)),
+            dma((chips, parts - 1)),
+            dma((chips, parts - 1)),
+            dma((chips,)),
+            dma((chips,)),
+        ],
+        compiler_params=pltpu.CompilerParams(collective_id=2, has_side_effects=True),
+        name="sum_rows",
+    )(partial.astype(BF16).reshape(n, parts, rows, model), residual)
 
 
 def solution(mesh):

time: 296 us -> 148 us (0.50)
  waiting for transfers between devices: 208 us -> 0 us
  Pallas kernels: 40.8 us -> 112 us
  between operations: 13.5 us -> 0.08 us
  matrix products: 18.3 us -> 24.6 us
    reduce_scatter x1 -> x0, waiting for transfers between devices: 142 us -> none  [on_device(): lax.psum_scatter(partial.astype(BF16).reshape(n * seq_rows, model), ('sp'...]
    pallas_call x0 -> x2, Pallas kernels: none -> 71.2 us  [the longest x1 37.3 us: on_device(): pl.pallas_call(functools.partial(gather_kernel, n, parts), out_shape=jax....]
    all_gather x1 -> x0, waiting for transfers between devices: 65.6 us -> none  [on_device(): every = lax.all_gather(normed, ('sp', 'tp'), axis=0, tiled=True)]
    dot_general x2, matrix products: 4.14 us -> 9.32 us  [ffn(): gate = jnp.dot(x, wg, preferred_element_type=F32)]
  transfers between devices with their start and end apart: 2 -> 0, of which waited for: 2 -> 0; matrix products, arithmetic and copies ran while one was open for 0% -> 0% of each run, Pallas kernels for 0% -> 0%
where the time goes in v2:
time: 148 us; the launch traced here: 147 us
  Pallas kernels  112 us (76%)
  matrix products  24.6 us (17%)
  local copies, waits for them, and re-layouts  7.31 us (5%)
  other arithmetic  3.58 us (2%)
    pallas_call x1, Pallas kernels, on_device(): pl.pallas_call(functools.partial(mixer_kernel, n, parts, groups), out_sha...  40.6 us
    pallas_call x1, Pallas kernels, on_device(): pl.pallas_call(functools.partial(gather_kernel, n, parts), out_shape=jax....  37.3 us
    pallas_call x1, Pallas kernels, on_device(): pl.pallas_call(functools.partial(sum_kernel, n, parts), out_shape=jax.Sha...  33.9 us
    dot_general x2, matrix products, ffn(): gate = jnp.dot(x, wg, preferred_element_type=F32)  9.32 us
    dot_general x2, matrix products, ffn(): return jnp.dot(hidden.astype(BF16), wd, preferred_element_type=F32)  8.72 us
    dot_general x1, matrix products, ffn(): up = jnp.dot(x, wu, preferred_element_type=F32)  6.53 us

profile of v2, /device:TPU:0, one launch (start us, length us, event | category | flops | bytes accessed | tf_op | source)
XLA Modules:
  0.0 147.3 jit_solution(1284058911759563675)
XLA Ops:
  0.0 0.0 copy-start
  0.0 1.2 constant_dynamic-slice_fusion.1
  1.2 0.1 copy.36
  1.4 0.1 copy.33
  1.5 1.6 %pad_maximum_fusion.joined_ref = bf16[128,768]{1,0:T(8,128)(2,1)} fusion(bf16[128,256]{1,0:T(8,128)(2,1)S(1)} %copy.33, bf16[128,512]{1,0:T(8,128)(2,1)} %param.22), kind=kLoop, calls=%fused_computation.18 | loop fusion | flops 393216 | bytes 393216 | tf_op jit(solution)/shard_map/concatenate | solution.py:479
  3.1 0.8 dynamic-slice_reduce_fusion
  3.8 0.6 copy.39
  4.4 0.7 bitcast_convert_fusion
  5.1 0.7 copy.34.pre_ref
  5.9 1.4 copy.35.spike_ref
  7.3 1.3 select_reduce_fusion.route_ref
  8.6 40.6 %mixer.1 = (bf16[32,2048]{1,0:T(8,128)(2,1)}, bf16[32,2048]{1,0:T(8,128)(2,1)}, f32[8,8,128]{2,1,0:T(8,128)}) custom-call(bf16[128,768]{1,0:T(8,128)(2,1)} %pad_maximum_fusion.joined_ref, f32[5,512]{1,0:T(8,128)} %value_taps_ref.1, f32[5,256]{1,0:T(8,128)} %bitcast.39, f32[128,16]{1,0:T(8,128)} %copy.34.pre_ref, f32[128,16]{1,0:T(8,128)} %copy.35.spike_ref, ...), custom_call_target="tpu_custom_call" | custom-call | tf_op jit(solution)/shard_map/mixer/pallas_call | solution.py:487
  49.2 37.3 %gather_rows.1 = bf16[8,4,32,2048]{3,2,1,0:T(8,128)(2,1)} custom-call(bf16[32,2048]{1,0:T(8,128)(2,1)} %get-tuple-element.8.x_ref), custom_call_target="tpu_custom_call" | custom-call | tf_op jit(solution)/shard_map/gather_rows/pallas_call | solution.py:531
  86.5 6.5 %fusion.1 = f32[1024,512]{1,0:T(8,128)} fusion(bf16[1024,2048]{1,0:T(8,128)(2,1)} %bitcast.33, bf16[1,2048,512]{2,1,0:T(8,128)(2,1)} %param.37), kind=kOutput, calls=%fused_computation.2 | convolution fusion | flops 2147483648 | bytes 8388608 | tf_op jit(solution)/shard_map/dot_general | solution.py:552
  93.0 0.8 constant_dynamic-slice_fusion
  93.8 7.1 %multiply_convert_fusion = bf16[1024,512]{1,0:T(8,128)(2,1)} fusion(f32[1024,512]{1,0:T(8,128)} %fusion.1, bf16[1024,2048]{1,0:T(8,128)(2,1)} %bitcast.34, bf16[1,2048,512]{2,1,0:T(8,128)(2,1)} %param.36, f32[1024]{0:T(1024)S(1)} %bitcast.43), kind=kOutput, calls=%fused_computation.6 | convolution fusion | flops 2151153664 | bytes 9441280 | tf_op jit(solution)/shard_map/dot_general | solution.py:551
  100.9 2.2 %fusion.11 = f32[128,512]{1,0:T(8,128)S(1)} fusion(bf16[2048,512]{1,0:T(8,128)(2,1)} %param.39, bf16[1024,2048]{1,0:T(8,128)(2,1)} %bitcast.35, s32[]{:T(128)S(6)} %select_n.27), kind=kOutput, calls=%fused_computation.11 | convolution fusion | flops 268435456 | bytes 2883588 | tf_op jit(solution)/shard_map/dot_general | solution.py:551
  103.1 3.2 %fusion.8 = f32[128,2048]{1,0:T(8,128)S(1)} fusion(bf16[512,2048]{1,0:T(8,128)(2,1)} %param.41, bf16[2048,512]{1,0:T(8,128)(2,1)} %param.40, bf16[1024,2048]{1,0:T(8,128)(2,1)} %bitcast.36, s32[]{:T(128)S(6)} %select_n.27, f32[128,512]{1,0:T(8,128)S(1)} %fusion.11), kind=kOutput, calls=%fused_computation.9 | convolution fusion | flops 537264128 | bytes 6029316 | tf_op jit(solution)/shard_map/dot_general | solution.py:556
  106.4 0.0 copy-done
  106.4 5.5 %add_convert_fusion = bf16[8,128,2048]{2,1,0:T(8,128)(2,1)} fusion(f32[128,2048]{1,0:T(8,128)S(1)} %fusion.8, pred[8]{0:T(512)(128)(4,1)S(1)} %iota_compare_fusion.1, bf16[8,128,512]{2,1,0:T(8,128)(2,1)} %bitcast.45, bf16[1,512,2048]{2,1,0:T(8,128)(2,1)S(1)} %copy-done), kind=kOutput, calls=%fused_computation | convolution fusion | flops 2153775104 | bytes 8388616 | tf_op jit(solution)/shard_map/dot_general | solution.py:556
  111.9 33.9 %sum_rows.1 = bf16[32,2048]{1,0:T(8,128)(2,1)} custom-call(bf16[8,4,32,2048]{3,2,1,0:T(8,128)(2,1)} %bitcast.37, bf16[32,2048]{1,0:T(8,128)(2,1)} %get-tuple-element.10.resid_ref), custom_call_target="tpu_custom_call" | custom-call | tf_op jit(solution)/shard_map/sum_rows/pallas_call | solution.py:570
  145.8 1.6 %copy.41 = bf16[32,2048]{1,0:T(8,128)(2,1)} copy(bf16[32,2048]{1,0:T(8,128)(2,1)} %sum_rows.1) | data formatting | bytes 262144
  (1 shorter events, 0.0 us)
Async XLA Ops:
  0.0 106.4 %copy-start = (bf16[1,512,2048]{2,1,0:T(8,128)(2,1)S(1)}, bf16[1,512,2048]{2,1,0:T(8,128)(2,1)}, u32[]{:S(2)}) copy-start(bf16[1,512,2048]{2,1,0:T(8,128)(2,1)} %param.38) | copy-start | bytes 6291460
